TPU v7x, 32 devices: a whole 2x2x4 slice. The times are simulated.
32 devices in a mesh: ep: 8 (over z, x), tp: 4 (over y, core).
Axes of the slice: x: 2, y: 2, z: 4, core: 2. Of those that a mesh axis runs over, the one named last changes fastest.
Arguments:
- queries: bfloat16 [2048, 2048], P('ep', 'tp'), may hold values from -9 to 9
- keys: bfloat16 [2048, 2048], P('ep', 'tp'), may hold values from -9 to 9
- values: bfloat16 [2048, 2048], P('ep', 'tp'), may hold values from -6 to 6
- lambdas: float32 [16], P('tp'), may hold values from 0.3 to 0.8
- head_gain: float32 [128], replicated, may hold values from 0.1 to 1.9
- moe_input: bfloat16 [4096, 2048], P('ep'), may hold values from -6 to 6
- ffn_gain: float32 [2048], replicated, may hold values from 0.1 to 1.9
- group_router: bfloat16 [2048, 4], replicated, may hold values from -0.125 to 0.125
- expert_router: bfloat16 [2048, 8], replicated, may hold values from -0.125 to 0.125
- routes: int32 [4096, 2], P('ep'), may hold values from 0 to 7, as said below
- w_gate: bfloat16 [8, 2048, 1024], P('ep', None, 'tp'), may hold values from -0.125 to 0.125
- w_up: bfloat16 [8, 2048, 1024], P('ep', None, 'tp'), may hold values from -0.125 to 0.125
- w_down: bfloat16 [8, 1024, 2048], P('ep', 'tp'), may hold values from -0.1875 to 0.1875
Outputs:
- attn_out: bfloat16 [2048, 2048], P('ep', 'tp')
- moe_out: bfloat16 [4096, 2048], P(('ep', 'tp'))
Inputs may be any that keep to these rules, and one draw needn't show every extreme that they name: `routes`: in each aligned block of 128 rows (the rows of one device) every expert is named by exactly 32 rows and every group by the same number of rows; a row's two experts differ and lie in one group of 2 consecutive expert numbers.
All inputs are finite; a program needn't handle non-finite values.
Results may differ from a plain program's by a relative error of at most 0.015.
Values may be sent and summed in bfloat16 or wider, within the bound.
A program may use at most 128 MiB of HBM per device.

v0:
```python
import math

import jax
import jax.numpy as jnp
from jax import lax
from jax.sharding import PartitionSpec as P

norm_eps = 1e-06
masked_score = -1e30


def rms_scaled(rows, gain):
    widened = rows.astype(jnp.float32)
    return (
        widened * lax.rsqrt(jnp.mean(widened * widened, axis=-1, keepdims=True) + norm_eps) * gain
    )


def score_block(query_heads, key_rows, score_scale):
    key_heads = key_rows.reshape(key_rows.shape[0], query_heads.shape[1], 2, query_heads.shape[3])
    return (
        jnp.einsum("qhmd,khmd->hmqk", query_heads, key_heads, preferred_element_type=jnp.float32)
        * score_scale
    )


def route_gates(normed, own_routes, group_router, expert_router):
    group_count = group_router.shape[1]
    expert_count = expert_router.shape[1]
    group_logits = jnp.dot(normed, group_router, preferred_element_type=jnp.float32)
    expert_logits = jnp.dot(normed, expert_router, preferred_element_type=jnp.float32)
    chosen = own_routes[:, 0] // (expert_count // group_count)
    group_mask = jnp.arange(group_count, dtype=jnp.int32)[None, :] == chosen[:, None]
    own_logit = jnp.sum(jnp.where(group_mask, group_logits, 0.0), axis=-1, keepdims=True)
    group_share = 1.0 / jnp.sum(jnp.exp(group_logits - own_logit), axis=-1)
    expert_mask = jnp.arange(expert_count, dtype=jnp.int32)[None, None, :] == own_routes[:, :, None]
    picked = jnp.sum(jnp.where(expert_mask, expert_logits[:, None, :], 0.0), axis=-1)
    return group_share[:, None] * jax.nn.sigmoid(picked - picked[:, ::-1])


def slot_places(own_routes, expert_count, capacity):
    flat_routes = own_routes.reshape(-1)
    one_hot = (flat_routes[:, None] == jnp.arange(expert_count, dtype=jnp.int32)[None, :]).astype(
        jnp.int32
    )
    earlier = jnp.cumsum(one_hot, axis=0) - one_hot
    return flat_routes * capacity + jnp.sum(earlier * one_hot, axis=1)


def dispatch_rows(normed_rows, own_routes, expert_count, capacity):
    places = slot_places(own_routes, expert_count, capacity)
    owners = jnp.arange(places.shape[0], dtype=jnp.int32) // 2
    holder = jnp.zeros((expert_count * capacity,), jnp.int32).at[places].set(owners)
    return normed_rows[holder].reshape(expert_count, capacity, normed_rows.shape[1])


def local(
    queries,
    keys,
    values,
    lambdas,
    head_gain,
    moe_input,
    ffn_gain,
    group_router,
    expert_router,
    routes,
    w_gate,
    w_up,
    w_down,
):
    query_count = queries.shape[0]
    heads_here = lambdas.shape[0]
    value_width = values.shape[1] // heads_here
    qk_width = queries.shape[1] // (2 * heads_here)
    query_heads = queries.reshape(query_count, heads_here, 2, qk_width)
    score_scale = qk_width ** (-0.5)
    query_first = lax.axis_index("ep") * query_count
    query_pos = query_first + jnp.arange(query_count, dtype=jnp.int32)
    query_last = query_first + query_count - 1
    stats_start = (
        jnp.full((heads_here, 2, query_count), masked_score, jnp.float32),
        jnp.zeros((heads_here, 2, query_count), jnp.float32),
    )
    key_shard = lax.all_gather(keys, "ep", axis=0, tiled=True)
    block_rows = math.gcd(key_shard.shape[0], 512)

    def stats_sweep_step(number, current):
        offset = number * block_rows

        def stats_compute(running):
            maxima, totals = running
            key_pos = offset + jnp.arange(block_rows, dtype=jnp.int32)
            allowed = key_pos[None, :] <= query_pos[:, None]
            key_block = lax.dynamic_slice_in_dim(key_shard, offset, block_rows, 0)
            scores = jnp.where(
                allowed, score_block(query_heads, key_block, score_scale), masked_score
            )
            new_max = jnp.maximum(maxima, jnp.max(scores, axis=-1))
            weights = jnp.where(allowed, jnp.exp(scores - new_max[..., None]), 0.0)
            return (new_max, totals * jnp.exp(maxima - new_max) + jnp.sum(weights, axis=-1))

        return lax.cond(offset <= query_last, stats_compute, lambda running: running, current)

    maxima, totals = lax.fori_loop(
        0, key_shard.shape[0] // block_rows, stats_sweep_step, stats_start
    )
    value_key_shard = lax.all_gather(keys, "ep", axis=0, tiled=True)
    value_shard = lax.all_gather(values, "ep", axis=0, tiled=True)
    value_block_rows = math.gcd(value_key_shard.shape[0], 512)

    def value_sweep_step(number, current):
        offset = number * value_block_rows

        def value_compute(running):
            key_pos = offset + jnp.arange(value_block_rows, dtype=jnp.int32)
            allowed = key_pos[None, :] <= query_pos[:, None]
            key_block = lax.dynamic_slice_in_dim(value_key_shard, offset, value_block_rows, 0)
            scores = score_block(query_heads, key_block, score_scale)
            shares = (
                jnp.where(allowed, jnp.exp(scores - maxima[..., None]), 0.0) / totals[..., None]
            )
            mixed = (shares[:, 0] - lambdas[:, None, None] * shares[:, 1]).astype(jnp.bfloat16)
            value_rows = lax.dynamic_slice_in_dim(value_shard, offset, value_block_rows, 0).reshape(
                value_block_rows, heads_here, value_width
            )
            return running + jnp.einsum(
                "hqk,khd->hqd", mixed, value_rows, preferred_element_type=jnp.float32
            )

        return lax.cond(offset <= query_last, value_compute, lambda running: running, current)

    heads_out = lax.fori_loop(
        0,
        value_key_shard.shape[0] // value_block_rows,
        value_sweep_step,
        jnp.zeros((heads_here, query_count, value_width), jnp.float32),
    )
    attn_out = rms_scaled(heads_out, head_gain).astype(jnp.bfloat16)
    attn_out = attn_out.transpose(1, 0, 2).reshape(query_count, heads_here * value_width)
    tp_count = lax.axis_size("tp")
    tp_index = lax.axis_index("tp")
    own_count = routes.shape[0] // tp_count
    expert_count = expert_router.shape[1]
    capacity = 2 * own_count // expert_count
    model_width = moe_input.shape[1]
    own_routes = lax.dynamic_slice_in_dim(routes, tp_index * own_count, own_count, 0)
    gate_local = w_gate[0]
    up_local = w_up[0]
    down_local = w_down[0]
    own_input = lax.dynamic_slice_in_dim(moe_input, tp_index * own_count, own_count, 0)
    normed = rms_scaled(own_input, ffn_gain).astype(jnp.bfloat16)
    packed = dispatch_rows(normed, own_routes, expert_count, capacity)
    arrived = lax.all_to_all(packed, "ep", split_axis=0, concat_axis=0, tiled=True)
    arrived_rows = lax.all_gather(arrived.reshape(-1, model_width), "tp", axis=0, tiled=True)
    gate_part = jnp.dot(arrived_rows, gate_local, preferred_element_type=jnp.float32)
    up_part = jnp.dot(arrived_rows, up_local, preferred_element_type=jnp.float32)
    hidden = (jax.nn.silu(gate_part) * up_part).astype(jnp.bfloat16)
    summed = lax.psum_scatter(
        jnp.dot(hidden, down_local, preferred_element_type=jnp.float32).astype(jnp.bfloat16),
        "tp",
        scatter_dimension=0,
        tiled=True,
    )
    homed = lax.all_to_all(
        summed.reshape(expert_count, capacity, model_width),
        "ep",
        split_axis=0,
        concat_axis=0,
        tiled=True,
    )
    places = slot_places(own_routes, expert_count, capacity)
    returned = homed.reshape(expert_count * capacity, model_width)[places].reshape(
        own_count, 2, model_width
    )
    gates = route_gates(normed, own_routes, group_router, expert_router)
    moe_out = jnp.sum(returned.astype(jnp.float32) * gates[..., None], axis=1).astype(jnp.bfloat16)
    return (attn_out, moe_out)


def solution(mesh):
    in_specs = (
        P("ep", "tp"),
        P("ep", "tp"),
        P("ep", "tp"),
        P("tp"),
        P(),
        P("ep", None),
        P(),
        P(),
        P(),
        P("ep", None),
        P("ep", None, "tp"),
        P("ep", None, "tp"),
        P("ep", "tp", None),
    )
    out_specs = (P("ep", "tp"), P(("ep", "tp"), None))
    return jax.shard_map(local, mesh=mesh, in_specs=in_specs, out_specs=out_specs, check_vma=False)
```

profile of v0, /device:TPU:25, one launch (start us, length us, event | category | flops | bytes accessed | tf_op | source)
XLA Modules:
  0.0 235.7 jit_solution(4646205072305375631)
XLA Ops:
  8.1 0.8 broadcast_multiply_fusion
  9.2 1.2 fusion.12
  10.6 0.1 mul.134
  10.7 0.6 reduce-window.6
  11.3 0.2 slice_reduce_fusion
  11.7 1.4 scatter_custom_fusion
  13.1 1.3 fusion.14
  14.4 1.4 gather_fusion
  15.8 28.6 %all_to_all.10 = bf16[8,32,2048]{2,1,0:T(8,128)(2,1)} all-to-all(bf16[8,32,2048]{2,1,0:T(8,128)(2,1)S(1)} %bitcast.83), channel_id=1, replica_groups=mesh['ep'=8,'tp'=4] {'ep'}, dimensions={0} | all-to-all | bytes 2097152 | tf_op jit(solution)/shard_map/all_to_all | solution.py:154
  44.4 36.6 %all-gather.8.cloned.1.call-done = bf16[1024,2048]{1,0:T(8,128)(2,1)} async-done(((bf16[256,2048]{1,0:T(8,128)(2,1)}), bf16[1024,2048]{1,0:T(8,128)(2,1)}) %all-gather.8.cloned.1.call-update) | async-done | bytes 4194320 | tf_op jit(solution)/shard_map/all_gather | solution.py:155
  81.0 4.8 %fusion.18 = f32[1024,256]{1,0:T(8,128)} fusion(bf16[1024,2048]{1,0:T(8,128)(2,1)} %all-gather.8.cloned.1.call-done, bf16[1,2048,256]{2,1,0:T(8,128)(2,1)} %param.31), kind=kOutput, calls=%fused_computation.38 | convolution fusion | flops 1073741824 | bytes 6291456 | tf_op jit(solution)/shard_map/dot_general | solution.py:156
  85.9 8.8 %convolution_convert_fusion = bf16[1024,2048]{1,0:T(8,128)(2,1)} fusion(bf16[1024,2048]{1,0:T(8,128)(2,1)} %all-gather.8.cloned.1.call-done, bf16[1,256,2048]{2,1,0:T(8,128)(2,1)S(1)} %copy-done, bf16[1,2048,256]{2,1,0:T(8,128)(2,1)S(1)} %copy-done.8, f32[1024,256]{1,0:T(8,128)} %fusion.18), kind=kOutput, calls=%fused_computation.27 | convolution fusion | flops 2151153664 | bytes 11534336 | tf_op jit(solution)/shard_map/dot_general | solution.py:160
  94.7 0.8 copy-done.1
  95.6 0.8 copy.37
  96.5 0.8 copy.39
  97.5 0.2 fusion.34
  97.8 41.1 %reduce-scatter.2.cloned.1.call-done = bf16[256,2048]{1,0:T(8,128)(2,1)} async-done(((bf16[1024,2048]{1,0:T(8,128)(2,1)}), bf16[256,2048]{1,0:T(8,128)(2,1)}) %reduce-scatter.2.cloned.1.call-update) | async-done | bytes 1048592 | tf_op jit(solution)/shard_map/reduce_scatter | solution.py:159
  138.8 5.4 %all-to-all-start.1 = ((bf16[8,32,2048]{2,1,0:T(8,128)(2,1)}), bf16[8,32,2048]{2,1,0:T(8,128)(2,1)S(1)}, u32[]{:S(2)}, u32[]{:S(2)}) async-start(bf16[8,32,2048]{2,1,0:T(8,128)(2,1)} %bitcast.86), calls=%async_computation.2 | async-start | bytes 2097152 | tf_op jit(solution)/shard_map/all_to_all | solution.py:165
  144.3 0.3 select_reduce_fusion.2
  144.8 1.2 all-gather.4.cloned.1.call-done
  146.0 13.0 %while.33 = (s32[]{:T(128)}, f32[4,2,256]{2,1,0:T(2,128)S(1)}, f32[4,2,256]{2,1,0:T(2,128)S(1)}, s32[]{:T(128)}, bf16[2048,512]{0,1:T(8,128)(2,1)}, /*index=5*/b...) while((s32[]{:T(128)}, f32[4,2,256]{2,1,0:T(2,128)S(1)}, ...), condition=%wide.region_5.6_spmd.clone, body=%wide.region_0.5_spmd.clone.sunk | while | flops 142742272 | bytes 10731789 | solution.py:105
  146.0 3.2 %conditional.6 = ((f32[4,2,256]{2,1,0:T(2,128)S(1)}, f32[4,2,256]{2,1,0:T(2,128)S(1)})) conditional(s32[]{:T(128)} %convert_element_type.85, (f32[4,2,256]{2,1,0:T(2,128)S(1)}, f32[4,2,256]{2,1,0:T(2,128)S(1)}) %tuple.87, (s32[]{:T(128)}, s32[]{:T(128)}, bf16[2048,512]{0,1:T(8,128)(2,1)}, bf16[256,4,2,64]{0,3,2,1:T(8,128)(2,1)S(1)}, ...), branch_computations={%region_1.0_spmd, %region_2.4_spmd} | conditional | flops 142742272 | bytes 10730566 | solution.py:103
  146.1 0.1 broadcast_compare_fusion
  146.2 1.1 constant_dynamic-slice_fusion
  147.3 0.9 fusion.4
  148.2 1.0 select_reduce_fusion
  149.3 3.2 %conditional.6 = ((f32[4,2,256]{2,1,0:T(2,128)S(1)}, f32[4,2,256]{2,1,0:T(2,128)S(1)})) conditional(s32[]{:T(128)} %convert_element_type.85, (f32[4,2,256]{2,1,0:T(2,128)S(1)}, f32[4,2,256]{2,1,0:T(2,128)S(1)}) %tuple.87, (s32[]{:T(128)}, s32[]{:T(128)}, bf16[2048,512]{0,1:T(8,128)(2,1)}, bf16[256,4,2,64]{0,3,2,1:T(8,128)(2,1)S(1)}, ...), branch_computations={%region_1.0_spmd, %region_2.4_spmd} | conditional | flops 142742272 | bytes 10730566 | solution.py:103
  149.3 0.1 broadcast_compare_fusion
  149.5 1.1 constant_dynamic-slice_fusion
  150.6 0.9 fusion.4
  151.4 1.0 select_reduce_fusion
  152.5 3.2 %conditional.6 = ((f32[4,2,256]{2,1,0:T(2,128)S(1)}, f32[4,2,256]{2,1,0:T(2,128)S(1)})) conditional(s32[]{:T(128)} %convert_element_type.85, (f32[4,2,256]{2,1,0:T(2,128)S(1)}, f32[4,2,256]{2,1,0:T(2,128)S(1)}) %tuple.87, (s32[]{:T(128)}, s32[]{:T(128)}, bf16[2048,512]{0,1:T(8,128)(2,1)}, bf16[256,4,2,64]{0,3,2,1:T(8,128)(2,1)S(1)}, ...), branch_computations={%region_1.0_spmd, %region_2.4_spmd} | conditional | flops 142742272 | bytes 10730566 | solution.py:103
  152.6 0.1 broadcast_compare_fusion
  152.7 1.1 constant_dynamic-slice_fusion
  153.8 0.9 fusion.4
  154.7 1.0 select_reduce_fusion
  155.8 3.2 %conditional.6 = ((f32[4,2,256]{2,1,0:T(2,128)S(1)}, f32[4,2,256]{2,1,0:T(2,128)S(1)})) conditional(s32[]{:T(128)} %convert_element_type.85, (f32[4,2,256]{2,1,0:T(2,128)S(1)}, f32[4,2,256]{2,1,0:T(2,128)S(1)}) %tuple.87, (s32[]{:T(128)}, s32[]{:T(128)}, bf16[2048,512]{0,1:T(8,128)(2,1)}, bf16[256,4,2,64]{0,3,2,1:T(8,128)(2,1)S(1)}, ...), branch_computations={%region_1.0_spmd, %region_2.4_spmd} | conditional | flops 142742272 | bytes 10730566 | solution.py:103
  155.8 0.1 broadcast_compare_fusion
  156.0 1.1 constant_dynamic-slice_fusion
  157.1 0.9 fusion.4
  157.9 1.0 select_reduce_fusion
  159.0 44.9 %all-gather.6.cloned.1.call-done = bf16[2048,512]{0,1:T(8,128)(2,1)} async-done(((bf16[256,512]{0,1:T(8,128)(2,1)}), bf16[2048,512]{0,1:T(8,128)(2,1)}) %all-gather.6.cloned.1.call-update) | async-done | bytes 2097168 | tf_op jit(solution)/shard_map/all_gather | solution.py:109
  204.0 14.4 %while.34 = (s32[]{:T(128)}, f32[4,256,128]{2,1,0:T(8,128)S(1)}, s32[]{:T(128)}, bf16[2048,512]{0,1:T(8,128)(2,1)}, bf16[256,4,2,64]{0,3,2,1:T(8,128)(2,1)S(1)},...) while((s32[]{:T(128)}, f32[4,256,128]{2,1,0:T(8,128)S(1)}, ...), condition=%wide.region_9.10_spmd.clone, body=%wide.region_6.9_spmd.clone.sunk | while | flops 274465536 | bytes 13132077 | solution.py:133
  204.1 3.6 %conditional.7 = (f32[4,256,128]{2,1,0:T(8,128)S(1)}) conditional(s32[]{:T(128)} %convert_element_type.86, f32[4,256,128]{2,1,0:T(8,128)S(1)} %get-tuple-element.604, (s32[]{:T(128)}, s32[]{:T(128)}, bf16[2048,512]{0,1:T(8,128)(2,1)}, bf16[256,4,2,64]{0,3,2,1:T(8,128)(2,1)S(1)}, f32[4,2,256]{2,1,0:T(2,128)S(1)}, ...), branch_computations={%region_7.7_spmd, %region_8.8_spmd} | conditional | flops 274465536 | bytes 13130822 | solution.py:131
  204.1 1.3 constant_dynamic-slice_fusion.1
  205.5 1.2 fusion.5
  206.8 0.8 convolution_add_fusion
  207.6 3.6 %conditional.7 = (f32[4,256,128]{2,1,0:T(8,128)S(1)}) conditional(s32[]{:T(128)} %convert_element_type.86, f32[4,256,128]{2,1,0:T(8,128)S(1)} %get-tuple-element.604, (s32[]{:T(128)}, s32[]{:T(128)}, bf16[2048,512]{0,1:T(8,128)(2,1)}, bf16[256,4,2,64]{0,3,2,1:T(8,128)(2,1)S(1)}, f32[4,2,256]{2,1,0:T(2,128)S(1)}, ...), branch_computations={%region_7.7_spmd, %region_8.8_spmd} | conditional | flops 274465536 | bytes 13130822 | solution.py:131
  207.7 1.3 constant_dynamic-slice_fusion.1
  209.1 1.2 fusion.5
  210.4 0.8 convolution_add_fusion
  211.2 3.6 %conditional.7 = (f32[4,256,128]{2,1,0:T(8,128)S(1)}) conditional(s32[]{:T(128)} %convert_element_type.86, f32[4,256,128]{2,1,0:T(8,128)S(1)} %get-tuple-element.604, (s32[]{:T(128)}, s32[]{:T(128)}, bf16[2048,512]{0,1:T(8,128)(2,1)}, bf16[256,4,2,64]{0,3,2,1:T(8,128)(2,1)S(1)}, f32[4,2,256]{2,1,0:T(2,128)S(1)}, ...), branch_computations={%region_7.7_spmd, %region_8.8_spmd} | conditional | flops 274465536 | bytes 13130822 | solution.py:131
  211.3 1.3 constant_dynamic-slice_fusion.1
  212.7 1.2 fusion.5
  214.0 0.8 convolution_add_fusion
  214.8 3.6 %conditional.7 = (f32[4,256,128]{2,1,0:T(8,128)S(1)}) conditional(s32[]{:T(128)} %convert_element_type.86, f32[4,256,128]{2,1,0:T(8,128)S(1)} %get-tuple-element.604, (s32[]{:T(128)}, s32[]{:T(128)}, bf16[2048,512]{0,1:T(8,128)(2,1)}, bf16[256,4,2,64]{0,3,2,1:T(8,128)(2,1)S(1)}, f32[4,2,256]{2,1,0:T(2,128)S(1)}, ...), branch_computations={%region_7.7_spmd, %region_8.8_spmd} | conditional | flops 274465536 | bytes 13130822 | solution.py:131
  214.9 1.3 constant_dynamic-slice_fusion.1
  216.3 1.2 fusion.5
  217.6 0.8 convolution_add_fusion
  218.4 0.2 multiply_reduce_fusion.1
  218.7 0.9 copy_bitcast_fusion
  219.6 2.3 gather_fusion.1
  221.9 2.4 %reshape.127 = f32[128,2,2048]{2,1,0:T(2,128)S(1)} reshape(bf16[256,2048]{1,0:T(8,128)(2,1)} %gather_fusion.1) | data formatting | bytes 3145728 | tf_op jit(solution)/shard_map/convert_element_type | solution.py:177
  224.3 3.9 %multiply_reduce_fusion = bf16[128,2048]{1,0:T(8,128)(2,1)} fusion(f32[128,2,2048]{2,1,0:T(2,128)S(1)} %reshape.127, f32[128,2]{1,0:T(8,128)S(1)} %copy.44), kind=kLoop, calls=%fused_computation.28 | loop fusion | flops 786432 | bytes 2622464 | tf_op jit(solution)/shard_map/reduce_sum | solution.py:177
  (92 shorter events, 2.1 us)
Async XLA Ops:
  8.0 77.9 %copy-start = (bf16[1,256,2048]{2,1,0:T(8,128)(2,1)S(1)}, bf16[1,256,2048]{2,1,0:T(8,128)(2,1)}, u32[]{:S(2)}) copy-start(bf16[1,256,2048]{2,1,0:T(8,128)(2,1)} %param.33) | copy-start | bytes 3145732
  8.0 73.0 %all-gather.8.cloned.1.call-start = ((), (), s32[]{:S(2)}) async-start(), calls=%async_computation.5 | async-start | bytes 5242880 | tf_op jit(solution)/shard_map/all_gather | solution.py:155
  44.3 41.5 %copy-start.8 = (bf16[1,2048,256]{2,1,0:T(8,128)(2,1)S(1)}, bf16[1,2048,256]{2,1,0:T(8,128)(2,1)}, u32[]{:S(2)}) copy-start(bf16[1,2048,256]{2,1,0:T(8,128)(2,1)} %param.32) | copy-start | bytes 3145732
  44.4 94.5 %reduce-scatter.2.cloned.1.call-start = ((), (), s32[]{:S(2)}) async-start(), calls=%async_computation.6 | async-start | bytes 5242880 | tf_op jit(solution)/shard_map/reduce_scatter | solution.py:159
  94.6 0.9 copy-start.1
  94.6 1.9 copy-start.2
  94.6 2.7 %copy-start.3 = (bf16[256,512]{1,0:T(8,128)(2,1)S(1)}, bf16[256,512]{1,0:T(8,128)(2,1)}, u32[]{:S(2)}) copy-start(bf16[256,512]{1,0:T(8,128)(2,1)} %param.21) | copy-start | bytes 786436
  94.6 2.9 %copy-start.4 = (bf16[2048,8]{0,1:T(8,128)(2,1)S(1)}, bf16[2048,8]{0,1:T(8,128)(2,1)}, u32[]{:S(2)}) copy-start(bf16[2048,8]{0,1:T(8,128)(2,1)} %param.29) | copy-start | bytes 98308
  94.6 49.7 %copy-start.5 = (bf16[2048,4]{0,1:T(4,128)(2,1)S(1)}, bf16[2048,4]{0,1:T(4,128)(2,1)}, u32[]{:S(2)}) copy-start(bf16[2048,4]{0,1:T(4,128)(2,1)} %param.28) | copy-start | bytes 49156
  94.7 51.3 %all-gather.4.cloned.1.call-start = ((), (), s32[]{:S(2)}) async-start(), calls=%async_computation.3 | async-start | bytes 2359296 | tf_op jit(solution)/shard_map/all_gather | solution.py:108
  96.4 107.5 %all-gather.6.cloned.1.call-start = ((), (), s32[]{:S(2)}) async-start(), calls=%async_computation.4 | async-start | bytes 2359296 | tf_op jit(solution)/shard_map/all_gather | solution.py:109
  138.8 80.8 %all-to-all-start.1 = ((bf16[8,32,2048]{2,1,0:T(8,128)(2,1)}), bf16[8,32,2048]{2,1,0:T(8,128)(2,1)S(1)}, u32[]{:S(2)}, u32[]{:S(2)}) async-start(bf16[8,32,2048]{2,1,0:T(8,128)(2,1)} %bitcast.86), calls=%async_computation.2 | async-start | bytes 2097152 | tf_op jit(solution)/shard_map/all_to_all | solution.py:165
  146.0 58.0 %copy-start.6 = (f32[4]{0:T(128)S(1)}, f32[4]{0:T(128)}, u32[]{:S(2)}) copy-start(f32[4]{0:T(128)} %param.24) | copy-start | bytes 52
  204.0 14.6 %copy-start.7 = (f32[128]{0:T(128)S(1)}, f32[128]{0:T(128)}, u32[]{:S(2)}) copy-start(f32[128]{0:T(128)} %param.25) | copy-start | bytes 1540
Sparse Core Ops, SparseCore 0:
  44.5 36.4 all-gather.7
  94.8 43.9 reduce-scatter.1
Sparse Core Ops, SparseCore 1:
  97.8 48.2 all-gather.3
  148.5 55.4 all-gather.5
where the time goes:
time: 236 us
  waiting for transfers between devices  124 us (53%)
  blocking collectives  28.6 us (12%)
  matrix products  25.8 us (11%)
  local copies, waits for them, and re-layouts  20.7 us (9%)
  between operations  15.7 us (7%)
  other arithmetic  14.5 us (6%)
  starting transfers between devices  5.61 us (2%)
    all_gather x1, waiting for transfers between devices, local(): value_shard = lax.all_gather(values, 'ep', axis=0, tiled=True)  44.9 us
    reduce_scatter x1, waiting for transfers between devices, local(): lax.psum_scatter(jnp.dot(hidden, down_local, preferred_element_type=jnp.f...  41.1 us
    all_gather x1, waiting for transfers between devices, local(): lax.all_gather(arrived.reshape(-1, model_width), 'tp', axis=0, tiled=True)  36.6 us
    all_to_all x1, blocking collectives, local(): lax.all_to_all(packed, 'ep', split_axis=0, concat_axis=0, tiled=True)  28.6 us
    dot_general x1, matrix products, local(): jnp.dot(hidden, down_local, preferred_element_type=jnp.float32)  8.75 us
    dot_general x8, matrix products, score_block(): jnp.einsum('qhmd,khmd->hmqk', query_heads, key_heads, preferred_element_t...  8.44 us
    all_to_all x1, starting transfers between devices, local(): lax.all_to_all(summed.reshape(expert_count, capacity, model_width), 'ep',...  5.44 us
    dynamic_slice x4, local copies, waits for them, and re-layouts, value_compute(): lax.dynamic_slice_in_dim(value_shard, offset, value_block_rows, 0)  5.11 us
  transfers between devices with their start and end apart: 5, of which 4 were waited for; matrix products, arithmetic and copies ran while one was open for 13% of the time, Pallas kernels for 0%

commit v1 on v0

--- a/solution.py
+++ b/solution.py
@@ -1,8 +1,11 @@
+import functools
 import math
 
 import jax
 import jax.numpy as jnp
 from jax import lax
+from jax.experimental import pallas as pl
+from jax.experimental.pallas import tpu as pltpu
 from jax.sharding import PartitionSpec as P
 
 norm_eps = 1e-06
@@ -178,6 +181,502 @@
     return (attn_out, moe_out)
 
 
+class Copies:
+    def __init__(self, send_sems, recv_sems):
+        self.send_sems = send_sems
+        self.recv_sems = recv_sems
+        self.made = []
+
+    def new(self, source, target, device):
+        number = len(self.made)
+        copy = pltpu.make_async_remote_copy(
+            src_ref=source,
+            dst_ref=target,
+            send_sem=self.send_sems.at[number],
+            recv_sem=self.recv_sems.at[number],
+            device_id=device,
+            device_id_type=pl.DeviceIdType.MESH,
+        )
+        copy.start()
+        self.made.append(copy)
+        return copy
+
+    def drain(self):
+        for copy in self.made:
+            copy.wait_send()
+
+
+def fused_kernel(
+    groups,
+    score_scale,
+    queries,
+    keys,
+    values,
+    lambdas,
+    head_gain,
+    moe_input,
+    ffn_gain,
+    router,
+    routes,
+    w_gate,
+    w_up,
+    w_down,
+    attn_out,
+    moe_out,
+    own_rows,
+    packed,
+    rows,
+    gate_w,
+    up_w,
+    down_w,
+    half_out,
+    half_in,
+    sums,
+    corner_out,
+    corner_in,
+    side_out,
+    side_in,
+    done,
+    returned,
+    q_all,
+    k_all,
+    v_all,
+    heads_done,
+    heads_back,
+    local_sems,
+    send_sems,
+    recv_sems,
+):
+    own_count, model_width = own_rows.shape
+    chunk = own_count // groups
+    half = chunk // 2
+    token_block, head_width = q_all.shape[1:]
+    ep = lax.axis_index("ep")
+    tp = lax.axis_index("tp")
+    plane, member = ep // 2, ep % 2
+    row, core = tp // 2, tp % 2
+    member_peer = (plane * 2 + (1 - member), tp)
+    row_peer = (ep, (1 - row) * 2 + core)
+    core_peer = (ep, row * 2 + (1 - core))
+    ahead = [(plane + step) % groups for step in range(groups)]
+    behind = [(plane + groups - step) % groups for step in range(groups)]
+
+    def at_plane(number):
+        return (number * 2 + member, tp)
+
+    def head_columns(ref, number):
+        return ref.at[:, pl.ds(pl.multiple_of(number * head_width, head_width), head_width)]
+
+    loads = []
+    for source, target in (
+        (moe_input.at[pl.ds(pl.multiple_of(tp * own_count, own_count), own_count)], own_rows),
+        (head_columns(queries, plane), q_all.at[plane]),
+        (head_columns(keys, plane), k_all.at[ep]),
+        (head_columns(values, plane), v_all.at[ep]),
+        (w_gate.at[0], gate_w),
+        (w_up.at[0], up_w),
+        (w_down.at[0], down_w),
+    ):
+        load = pltpu.make_async_copy(source, target, local_sems.at[len(loads)])
+        load.start()
+        loads.append(load)
+
+    barrier = pltpu.get_barrier_semaphore()
+    partners = [member_peer, row_peer, core_peer] + [at_plane(p) for p in ahead[1:]]
+    for partner in partners:
+        pl.semaphore_signal(
+            barrier, inc=1, device_id=partner, device_id_type=pl.DeviceIdType.MESH
+        )
+
+    own_routes = routes[pl.ds(pl.multiple_of(tp * own_count, own_count), own_count), :]
+    lead = own_routes[:, 0:1]
+    lane = lax.broadcasted_iota(jnp.int32, (own_count, own_count), 1)
+    sub = lax.broadcasted_iota(jnp.int32, (own_count, own_count), 0)
+    turned = plane + lane
+    lane_group = jnp.where(turned >= groups, turned - groups, turned)
+    in_group = (lead >= lane_group * 2) & (lead < lane_group * 2 + 2) & (lane < groups)
+    one_hot = jnp.where(in_group, 1.0, 0.0)
+    below = jnp.where(lane < sub, 1.0, 0.0).astype(jnp.bfloat16)
+    earlier = jnp.dot(below, one_hot.astype(jnp.bfloat16), preferred_element_type=jnp.float32)
+    lane_start = (lane * chunk).astype(jnp.float32)
+    place = jnp.sum(one_hot * (earlier + lane_start), axis=1, keepdims=True)
+    slots = jnp.where(place == lane.astype(jnp.float32), 1.0, 0.0).astype(jnp.bfloat16)
+
+    loads[0].wait()
+    widened = own_rows[...].astype(jnp.float32)
+    normed = (
+        widened
+        * lax.rsqrt(jnp.mean(widened * widened, axis=-1, keepdims=True) + norm_eps)
+        * ffn_gain[...]
+    ).astype(jnp.bfloat16)
+    by_group = lax.dot_general(
+        slots, normed, (((0,), (0,)), ((), ())), preferred_element_type=jnp.float32
+    ).astype(jnp.bfloat16)
+    rows[0, 0:chunk, :] = by_group[0:chunk]
+    for step in range(1, groups):
+        packed[step] = by_group[step * chunk : (step + 1) * chunk]
+
+    pl.semaphore_wait(barrier, len(partners))
+    copies = Copies(send_sems, recv_sems)
+
+    def slot(step, number):
+        return rows.at[step, pl.ds(number * chunk, chunk)]
+
+    arriving = [None] * groups
+    for step in range(1, groups):
+        arriving[step] = copies.new(packed.at[step], slot(step, 0), at_plane(ahead[step]))
+    kv_arriving = [None] * groups
+    q_arriving = []
+
+    def send_heads(step):
+        target = at_plane(ahead[step])
+        kv_arriving[step] = [
+            copies.new(head_columns(keys, ahead[step]), k_all.at[ep], target),
+            copies.new(head_columns(values, ahead[step]), v_all.at[ep], target),
+        ]
+        q_arriving.append(
+            copies.new(head_columns(queries, ahead[step]), q_all.at[plane], target)
+        )
+
+    first = [None] * groups
+    second = [None] * groups
+    third = [None] * groups
+    crossed = [None] * groups
+    corner = [None] * groups
+    sides = [None] * groups
+    homed = []
+    kv_crossed = []
+
+    def spread(step):
+        if arriving[step] is not None:
+            arriving[step].wait_recv()
+        first[step] = [
+            copies.new(slot(step, 0), slot(step, 1), member_peer),
+            copies.new(slot(step, 0), slot(step, 2), row_peer),
+        ]
+        third[step] = [copies.new(slot(step, 0), slot(step, groups_in_half), core_peer)]
+
+    def forward(step):
+        upper = pl.ds(3 * chunk, half)
+        lower = pl.ds(3 * chunk + half, half)
+        first[step][0].wait_recv()
+        to_row = copies.new(
+            rows.at[step, pl.ds(chunk, half)], rows.at[step, upper], row_peer
+        )
+        third[step].append(copies.new(slot(step, 1), slot(step, 5), core_peer))
+        first[step][1].wait_recv()
+        to_member = copies.new(
+            rows.at[step, pl.ds(2 * chunk + half, half)], rows.at[step, lower], member_peer
+        )
+        third[step].append(copies.new(slot(step, 2), slot(step, 6), core_peer))
+        second[step] = [to_row, to_member]
+
+    def compute(step):
+        for copy in second[step]:
+            copy.wait_recv()
+        third[step].append(copies.new(slot(step, 3), slot(step, 7), core_peer))
+        for copy in third[step]:
+            copy.wait_recv()
+        if step == 0:
+            for load in loads[4:]:
+                load.wait()
+        block = rows[step]
+        logits = jnp.dot(block, router[...], preferred_element_type=jnp.float32)
+        column = lax.broadcasted_iota(jnp.int32, logits.shape, 1)
+
+        def pick(number):
+            return jnp.sum(jnp.where(column == number, logits, 0.0), axis=1, keepdims=True)
+
+        own_group = pick(plane)
+        terms = jnp.where(column < groups, jnp.exp(logits - own_group), 0.0)
+        share = 1.0 / jnp.sum(jnp.where(column < groups, terms, 0.0), axis=1, keepdims=True)
+        gap = pick(groups + ep) - pick(groups + plane * 2 + (1 - member))
+        gates = share / (1.0 + jnp.exp(-gap))
+        gate_part = jnp.dot(block, gate_w[...], preferred_element_type=jnp.float32)
+        up_part = jnp.dot(block, up_w[...], preferred_element_type=jnp.float32)
+        hidden = (gate_part / (1.0 + jnp.exp(-gate_part)) * up_part).astype(jnp.bfloat16)
+        out = jnp.dot(hidden, down_w[...], preferred_element_type=jnp.float32) * gates
+        half_out[step] = out[4 * chunk :].astype(jnp.bfloat16)
+        sums[step] = out[: 4 * chunk]
+        crossed[step] = copies.new(half_out.at[step], half_in.at[step], core_peer)
+
+    def reduce_corner(step):
+        crossed[step].wait_recv()
+        total = sums[step] + half_in[step].astype(jnp.float32)
+        sums[step] = total
+        corner_out[step] = total[3 * chunk :].astype(jnp.bfloat16)
+        corner[step] = [
+            copies.new(
+                corner_out.at[step, pl.ds(0, half)], corner_in.at[step, pl.ds(0, half)], row_peer
+            ),
+            copies.new(
+                corner_out.at[step, pl.ds(half, half)],
+                corner_in.at[step, pl.ds(half, half)],
+                member_peer,
+            ),
+        ]
+
+    def reduce_sides(step):
+        for copy in corner[step]:
+            copy.wait_recv()
+        added = corner_in[step].astype(jnp.float32)
+        total = sums[step]
+        side_out[step, 0:half, :] = (total[chunk : chunk + half] + added[:half]).astype(
+            jnp.bfloat16
+        )
+        side_out[step, half : half + chunk, :] = total[chunk + half : 2 * chunk + half].astype(
+            jnp.bfloat16
+        )
+        side_out[step, half + chunk :, :] = (total[2 * chunk + half : 3 * chunk] + added[half:]).astype(
+            jnp.bfloat16
+        )
+        sides[step] = [
+            copies.new(
+                side_out.at[step, pl.ds(0, chunk)], side_in.at[step, pl.ds(0, chunk)], member_peer
+            ),
+            copies.new(
+                side_out.at[step, pl.ds(chunk, chunk)],
+                side_in.at[step, pl.ds(chunk, chunk)],
+                row_peer,
+            ),
+        ]
+
+    def finish(step):
+        for copy in sides[step]:
+            copy.wait_recv()
+        arrived = side_in[step].astype(jnp.float32)
+        total = (sums[step][:chunk] + arrived[:chunk] + arrived[chunk:]).astype(jnp.bfloat16)
+        if step == 0:
+            returned[0] = total
+        else:
+            done[step] = total
+            homed.append(copies.new(done.at[step], returned.at[step], at_plane(behind[step])))
+
+    def cross_heads(step):
+        if step == 0:
+            loads[2].wait()
+            loads[3].wait()
+        else:
+            for copy in kv_arriving[step]:
+                copy.wait_recv()
+        block = behind[step] * 2 + member
+        kv_crossed.append(copies.new(k_all.at[block], k_all.at[block], member_peer))
+        kv_crossed.append(copies.new(v_all.at[block], v_all.at[block], member_peer))
+
+    def ready_heads():
+        loads[1].wait()
+        for copy in q_arriving + kv_crossed:
+            copy.wait_recv()
+
+    back = []
+    weight = lambdas[plane]
+    factor = score_scale * math.log2(math.e)
+
+    def attend(number):
+        query = q_all[number]
+        lanes = lax.broadcasted_iota(jnp.int32, query.shape, 1)
+        nothing = jnp.zeros_like(query)
+        maps = [
+            jnp.where(lanes < head_width // 2, query, nothing),
+            jnp.where(lanes >= head_width // 2, query, nothing),
+        ]
+        ends = [2 * number, 2 * number + 2]
+        parts = [(0, ends[0])] if number else []
+        parts.append((ends[0], ends[1]))
+        key_parts = [k_all[a:b].reshape((b - a) * token_block, head_width) for a, b in parts]
+        value_parts = [v_all[a:b].reshape((b - a) * token_block, head_width) for a, b in parts]
+        mixed = [None] * len(parts)
+        for index, part_query in enumerate(maps):
+            scores = [
+                lax.dot_general(
+                    part_query, k, (((1,), (1,)), ((), ())), preferred_element_type=jnp.float32
+                )
+                for k in key_parts
+            ]
+            at = lax.broadcasted_iota(jnp.int32, scores[-1].shape, 1)
+            own = lax.broadcasted_iota(jnp.int32, scores[-1].shape, 0) + member * token_block
+            scores[-1] = jnp.where(at <= own, scores[-1], masked_score)
+            maxima = functools.reduce(
+                jnp.maximum, [jnp.max(s, axis=1, keepdims=True) for s in scores]
+            )
+            terms = [jnp.exp2((s - maxima) * factor) for s in scores]
+            total = sum(jnp.sum(t, axis=1, keepdims=True) for t in terms)
+            share = 1.0 / total if index == 0 else -weight / total
+            for place_number, t in enumerate(terms):
+                piece = t * share
+                if index:
+                    piece = mixed[place_number] + piece
+                mixed[place_number] = piece
+        heads = sum(
+            jnp.dot(w.astype(jnp.bfloat16), v, preferred_element_type=jnp.float32)
+            for w, v in zip(mixed, value_parts)
+        )
+        scaled = (
+            heads
+            * lax.rsqrt(jnp.mean(heads * heads, axis=-1, keepdims=True) + norm_eps)
+            * head_gain[...]
+        )
+        heads_done[number] = scaled.astype(jnp.bfloat16)
+
+    def send_attended():
+        for step in range(1, groups):
+            back.append(
+                copies.new(
+                    heads_done.at[ahead[step]], heads_back.at[plane], at_plane(ahead[step])
+                )
+            )
+
+    groups_in_half = 4
+    spread(0)
+    cross_heads(0)
+    for step in range(1, groups):
+        send_heads(step)
+    forward(0)
+    spread(1)
+    compute(0)
+    forward(1)
+    spread(2)
+    reduce_corner(0)
+    compute(1)
+    cross_heads(1)
+    forward(2)
+    reduce_sides(0)
+    spread(3)
+    reduce_corner(1)
+    compute(2)
+    cross_heads(2)
+    forward(3)
+    finish(0)
+    reduce_sides(1)
+    reduce_corner(2)
+    cross_heads(3)
+    compute(3)
+    finish(1)
+    reduce_sides(2)
+    ready_heads()
+    attend(0)
+    reduce_corner(3)
+    attend(1)
+    finish(2)
+    reduce_sides(3)
+    attend(2)
+    finish(3)
+    attend(3)
+    send_attended()
+    for copy in homed:
+        copy.wait_recv()
+    gathered = returned[...].reshape(own_count, model_width)
+    moe_out[...] = jnp.dot(slots, gathered, preferred_element_type=jnp.float32).astype(
+        jnp.bfloat16
+    )
+    for copy in back:
+        copy.wait_recv()
+    for number in range(groups):
+        columns = slice(number * head_width, (number + 1) * head_width)
+        attn_out[:, columns] = jnp.where(
+            plane == number, heads_done[number], heads_back[number]
+        )
+    copies.drain()
+
+
+def fused_local(
+    queries,
+    keys,
+    values,
+    lambdas,
+    head_gain,
+    moe_input,
+    ffn_gain,
+    group_router,
+    expert_router,
+    routes,
+    w_gate,
+    w_up,
+    w_down,
+):
+    groups = group_router.shape[1]
+    token_block, width = queries.shape
+    head_width = width // groups
+    model_width = moe_input.shape[1]
+    own_count = moe_input.shape[0] // lax.axis_size("tp")
+    hidden_width = w_gate.shape[2]
+    chunk = own_count // groups
+    router = jnp.concatenate([group_router, expert_router], axis=1)
+    router = jnp.pad(router, ((0, 0), (0, -router.shape[1] % 128)))
+    bf16, f32 = jnp.bfloat16, jnp.float32
+    vmem = pl.BlockSpec(memory_space=pltpu.VMEM)
+    smem = pl.BlockSpec(memory_space=pltpu.SMEM)
+    hbm = pl.BlockSpec(memory_space=pl.ANY)
+    copy_count = 3 + 9 + 8 * groups + 5 * groups + 3 + 8 + 3
+    blocks = 2 * groups
+    return pl.pallas_call(
+        functools.partial(fused_kernel, groups, (head_width // 2) ** -0.5),
+        out_shape=(
+            jax.ShapeDtypeStruct((token_block, width), bf16),
+            jax.ShapeDtypeStruct((own_count, model_width), bf16),
+        ),
+        in_specs=[hbm, hbm, hbm, smem, vmem, hbm, vmem, vmem, vmem, hbm, hbm, hbm],
+        out_specs=(vmem, vmem),
+        scratch_shapes=[
+            pltpu.VMEM((own_count, model_width), bf16),
+            pltpu.VMEM((groups, chunk, model_width), bf16),
+            pltpu.VMEM((groups, 8 * chunk, model_width), bf16),
+            pltpu.VMEM((model_width, hidden_width), bf16),
+            pltpu.VMEM((model_width, hidden_width), bf16),
+            pltpu.VMEM((hidden_width, model_width), bf16),
+            pltpu.VMEM((groups, 4 * chunk, model_width), bf16),
+            pltpu.VMEM((groups, 4 * chunk, model_width), bf16),
+            pltpu.VMEM((groups, 4 * chunk, model_width), f32),
+            pltpu.VMEM((groups, chunk, model_width), bf16),
+            pltpu.VMEM((groups, chunk, model_width), bf16),
+            pltpu.VMEM((groups, 2 * chunk, model_width), bf16),
+            pltpu.VMEM((groups, 2 * chunk, model_width), bf16),
+            pltpu.VMEM((groups, chunk, model_width), bf16),
+            pltpu.VMEM((groups, chunk, model_width), bf16),
+            pltpu.VMEM((groups, token_block, head_width), bf16),
+            pltpu.VMEM((blocks, token_block, head_width), bf16),
+            pltpu.VMEM((blocks, token_block, head_width), bf16),
+            pltpu.VMEM((groups, token_block, head_width), bf16),
+            pltpu.VMEM((groups, token_block, head_width), bf16),
+            pltpu.SemaphoreType.DMA((7,)),
+            pltpu.SemaphoreType.DMA((copy_count,)),
+            pltpu.SemaphoreType.DMA((copy_count,)),
+        ],
+        compiler_params=pltpu.CompilerParams(
+            collective_id=0, has_side_effects=True, vmem_limit_bytes=62_000_000
+        ),
+    )(
+        queries,
+        keys,
+        values,
+        lambdas,
+        head_gain[None, :],
+        moe_input,
+        ffn_gain[None, :],
+        router,
+        routes,
+        w_gate,
+        w_up,
+        w_down,
+    )
+
+
+def chosen_local(*arguments):
+    queries, lambdas = arguments[0], arguments[3]
+    moe_input, group_router, expert_router = arguments[5], arguments[7], arguments[8]
+    groups, experts = group_router.shape[1], expert_router.shape[1]
+    fits = (
+        experts == 2 * groups
+        and lax.axis_size("ep") == experts
+        and lax.axis_size("tp") == 4
+        and groups == 4
+        and lambdas.shape[0] == groups
+        and queries.shape[1] == groups * 128
+        and moe_input.shape[0] // 4 == 128
+    )
+    return fused_local(*arguments) if fits else local(*arguments)
+
+
 def solution(mesh):
     in_specs = (
         P("ep", "tp"),
@@ -195,4 +694,5 @@
         P("ep", "tp", None),
     )
     out_specs = (P("ep", "tp"), P(("ep", "tp"), None))
-    return jax.shard_map(local, mesh=mesh, in_specs=in_specs, out_specs=out_specs, check_vma=False)
+    return jax.shard_map(
+        chosen_local, mesh=mesh, in_specs=in_specs, out_specs=out_specs, check_vma=False)

time: 236 us -> 78.2 us (0.33)
  the two profiles are of different devices: /device:TPU:25 before, /device:TPU:0 now
where the time goes in v1:
time: 78.2 us; the launch traced here: 77.8 us
  Pallas kernels  70.1 us (90%)
  local copies, waits for them, and re-layouts  6.29 us (8%)
    pallas_call x1, Pallas kernels, fused_local(): pl.pallas_call(functools.partial(fused_kernel, groups, (head_width // 2)...  70.1 us
    unnamed x3, local copies, waits for them, and re-layouts  5.09 us

profile of v1, /device:TPU:0, one launch (start us, length us, event | category | flops | bytes accessed | tf_op | source)
XLA Modules:
  0.0 77.8 jit_solution(13233085711470125844)
XLA Ops:
  0.6 0.8 %pad_maximum_fusion = bf16[2048,12]{0,1:T(8,128)(2,1)S(1)} fusion(bf16[2048,8]{0,1:T(8,128)(2,1)} %param.21, bf16[2048,4]{0,1:T(4,128)(2,1)} %param.20), kind=kLoop, calls=%fused_computation | loop fusion | flops 98304 | bytes 98304 | tf_op jit(solution)/shard_map/concatenate | solution.py:604
  1.4 1.5 %copy.19.routes = s32[512,2]{1,0:T(8,128)} copy(s32[512,2]{0,1:T(2,128)} %param.22) | data formatting | bytes 8192 | tf_op args[9]
  3.0 0.3 copy.18
  3.3 0.9 %pad.4.router = bf16[2048,128]{1,0:T(8,128)(2,1)} pad(bf16[2048,12]{1,0:T(8,128)(2,1)S(1)} %copy.18, bf16[]{:T(256)} %constant.2.clone.1), padding=0_0x0_116 | pad | bytes 573442 | tf_op jit(solution)/shard_map/jit(_pad)/pad | solution.py:605
  4.2 70.1 %shard_map.140 = (bf16[256,512]{1,0:T(8,128)(2,1)}, bf16[128,2048]{1,0:T(8,128)(2,1)}) custom-call(bf16[256,512]{1,0:T(8,128)(2,1)} %queries.1, bf16[256,512]{1,0:T(8,128)(2,1)} %keys.1, bf16[256,512]{1,0:T(8,128)(2,1)} %values.1, f32[4]{0:T(128)} %lambdas.1, f32[1,128]{1,0:T(1,128)} %bitcast.3, bf16[512,2048]{1,0:T(8,128)(2,1)} %moe_input.1, ...), custom_call_target="tpu_custom_call" | custom-call | tf_op jit(solution)/shard_map/pallas_call | solution.py:612
  74.3 1.7 %copy.22 = bf16[256,512]{1,0:T(8,128)(2,1)} copy(bf16[256,512]{1,0:T(8,128)(2,1)} %get-tuple-element.4) | data formatting | bytes 524288
  76.0 1.9 %copy.23 = bf16[128,2048]{1,0:T(8,128)(2,1)} copy(bf16[128,2048]{1,0:T(8,128)(2,1)} %get-tuple-element.5) | data formatting | bytes 1048576

commit v2 on v1

--- a/solution.py
+++ b/solution.py
@@ -216,7 +216,8 @@
     head_gain,
     moe_input,
     ffn_gain,
-    router,
+    group_router,
+    expert_router,
     routes,
     w_gate,
     w_up,
@@ -243,13 +244,17 @@
     v_all,
     heads_done,
     heads_back,
+    router,
     local_sems,
     send_sems,
     recv_sems,
+    back_send_sems,
+    back_recv_sems,
 ):
     own_count, model_width = own_rows.shape
+    expert_first = 16
     chunk = own_count // groups
-    half = chunk // 2
+    halves = [chunk if step % 2 == 0 else chunk // 2 for step in range(groups)]
     token_block, head_width = q_all.shape[1:]
     ep = lax.axis_index("ep")
     tp = lax.axis_index("tp")
@@ -258,8 +263,11 @@
     member_peer = (plane * 2 + (1 - member), tp)
     row_peer = (ep, (1 - row) * 2 + core)
     core_peer = (ep, row * 2 + (1 - core))
-    ahead = [(plane + step) % groups for step in range(groups)]
-    behind = [(plane + groups - step) % groups for step in range(groups)]
+    high, low = plane // 2, plane % 2
+    ahead = [
+        (high + step // 2) % 2 * 2 + (low + step % 2) % 2 for step in range(groups)
+    ]
+    behind = ahead
 
     def at_plane(number):
         return (number * 2 + member, tp)
@@ -288,19 +296,22 @@
             barrier, inc=1, device_id=partner, device_id_type=pl.DeviceIdType.MESH
         )
 
-    own_routes = routes[pl.ds(pl.multiple_of(tp * own_count, own_count), own_count), :]
-    lead = own_routes[:, 0:1]
+    lead = routes[0:1, pl.ds(pl.multiple_of(tp * own_count, own_count), own_count)]
     lane = lax.broadcasted_iota(jnp.int32, (own_count, own_count), 1)
     sub = lax.broadcasted_iota(jnp.int32, (own_count, own_count), 0)
-    turned = plane + lane
-    lane_group = jnp.where(turned >= groups, turned - groups, turned)
-    in_group = (lead >= lane_group * 2) & (lead < lane_group * 2 + 2) & (lane < groups)
+    sub_group = jnp.zeros_like(sub)
+    for step in range(groups):
+        sub_group = jnp.where(sub == step, ahead[step], sub_group)
+    in_group = (lead >= sub_group * 2) & (lead < sub_group * 2 + 2) & (sub < groups)
     one_hot = jnp.where(in_group, 1.0, 0.0)
-    below = jnp.where(lane < sub, 1.0, 0.0).astype(jnp.bfloat16)
-    earlier = jnp.dot(below, one_hot.astype(jnp.bfloat16), preferred_element_type=jnp.float32)
-    lane_start = (lane * chunk).astype(jnp.float32)
-    place = jnp.sum(one_hot * (earlier + lane_start), axis=1, keepdims=True)
-    slots = jnp.where(place == lane.astype(jnp.float32), 1.0, 0.0).astype(jnp.bfloat16)
+    before = jnp.where(sub < lane, 1.0, 0.0).astype(jnp.bfloat16)
+    earlier = jnp.dot(one_hot.astype(jnp.bfloat16), before, preferred_element_type=jnp.float32)
+    sub_start = (sub * chunk).astype(jnp.float32)
+    place = jnp.sum(one_hot * (earlier + sub_start), axis=0, keepdims=True)
+    slots = jnp.where(place == sub.astype(jnp.float32), 1.0, 0.0).astype(jnp.bfloat16)
+    router[...] = jnp.zeros_like(router)
+    router[0:groups, :] = group_router[...]
+    router[expert_first : expert_first + 2 * groups, :] = expert_router[...]
 
     loads[0].wait()
     widened = own_rows[...].astype(jnp.float32)
@@ -309,9 +320,7 @@
         * lax.rsqrt(jnp.mean(widened * widened, axis=-1, keepdims=True) + norm_eps)
         * ffn_gain[...]
     ).astype(jnp.bfloat16)
-    by_group = lax.dot_general(
-        slots, normed, (((0,), (0,)), ((), ())), preferred_element_type=jnp.float32
-    ).astype(jnp.bfloat16)
+    by_group = jnp.dot(slots, normed, preferred_element_type=jnp.float32).astype(jnp.bfloat16)
     rows[0, 0:chunk, :] = by_group[0:chunk]
     for step in range(1, groups):
         packed[step] = by_group[step * chunk : (step + 1) * chunk]
@@ -357,31 +366,37 @@
         third[step] = [copies.new(slot(step, 0), slot(step, groups_in_half), core_peer)]
 
     def forward(step):
-        upper = pl.ds(3 * chunk, half)
-        lower = pl.ds(3 * chunk + half, half)
+        half = halves[step]
         first[step][0].wait_recv()
-        to_row = copies.new(
-            rows.at[step, pl.ds(chunk, half)], rows.at[step, upper], row_peer
-        )
+        second[step] = [
+            copies.new(
+                rows.at[step, pl.ds(chunk, half)], rows.at[step, pl.ds(3 * chunk, half)], row_peer
+            )
+        ]
         third[step].append(copies.new(slot(step, 1), slot(step, 5), core_peer))
         first[step][1].wait_recv()
-        to_member = copies.new(
-            rows.at[step, pl.ds(2 * chunk + half, half)], rows.at[step, lower], member_peer
-        )
+        if half < chunk:
+            second[step].append(
+                copies.new(
+                    rows.at[step, pl.ds(2 * chunk + half, chunk - half)],
+                    rows.at[step, pl.ds(3 * chunk + half, chunk - half)],
+                    member_peer,
+                )
+            )
         third[step].append(copies.new(slot(step, 2), slot(step, 6), core_peer))
-        second[step] = [to_row, to_member]
-
-    def compute(step):
+
+    def pass_corner(step):
         for copy in second[step]:
             copy.wait_recv()
         third[step].append(copies.new(slot(step, 3), slot(step, 7), core_peer))
+
+    def compute(step):
         for copy in third[step]:
             copy.wait_recv()
-        if step == 0:
-            for load in loads[4:]:
-                load.wait()
         block = rows[step]
-        logits = jnp.dot(block, router[...], preferred_element_type=jnp.float32)
+        logits = lax.dot_general(
+            block, router[...], (((1,), (1,)), ((), ())), preferred_element_type=jnp.float32
+        )
         column = lax.broadcasted_iota(jnp.int32, logits.shape, 1)
 
         def pick(number):
@@ -390,7 +405,7 @@
         own_group = pick(plane)
         terms = jnp.where(column < groups, jnp.exp(logits - own_group), 0.0)
         share = 1.0 / jnp.sum(jnp.where(column < groups, terms, 0.0), axis=1, keepdims=True)
-        gap = pick(groups + ep) - pick(groups + plane * 2 + (1 - member))
+        gap = pick(expert_first + ep) - pick(expert_first + plane * 2 + (1 - member))
         gates = share / (1.0 + jnp.exp(-gap))
         gate_part = jnp.dot(block, gate_w[...], preferred_element_type=jnp.float32)
         up_part = jnp.dot(block, up_w[...], preferred_element_type=jnp.float32)
@@ -405,20 +420,25 @@
         total = sums[step] + half_in[step].astype(jnp.float32)
         sums[step] = total
         corner_out[step] = total[3 * chunk :].astype(jnp.bfloat16)
+        half = halves[step]
         corner[step] = [
             copies.new(
                 corner_out.at[step, pl.ds(0, half)], corner_in.at[step, pl.ds(0, half)], row_peer
-            ),
-            copies.new(
-                corner_out.at[step, pl.ds(half, half)],
-                corner_in.at[step, pl.ds(half, half)],
-                member_peer,
-            ),
+            )
         ]
+        if half < chunk:
+            corner[step].append(
+                copies.new(
+                    corner_out.at[step, pl.ds(half, chunk - half)],
+                    corner_in.at[step, pl.ds(half, chunk - half)],
+                    member_peer,
+                )
+            )
 
     def reduce_sides(step):
         for copy in corner[step]:
             copy.wait_recv()
+        half = halves[step]
         added = corner_in[step].astype(jnp.float32)
         total = sums[step]
         side_out[step, 0:half, :] = (total[chunk : chunk + half] + added[:half]).astype(
@@ -427,9 +447,10 @@
         side_out[step, half : half + chunk, :] = total[chunk + half : 2 * chunk + half].astype(
             jnp.bfloat16
         )
-        side_out[step, half + chunk :, :] = (total[2 * chunk + half : 3 * chunk] + added[half:]).astype(
-            jnp.bfloat16
-        )
+        if half < chunk:
+            side_out[step, half + chunk :, :] = (
+                total[2 * chunk + half : 3 * chunk] + added[half:]
+            ).astype(jnp.bfloat16)
         sides[step] = [
             copies.new(
                 side_out.at[step, pl.ds(0, chunk)], side_in.at[step, pl.ds(0, chunk)], member_peer
@@ -468,7 +489,6 @@
         for copy in q_arriving + kv_crossed:
             copy.wait_recv()
 
-    back = []
     weight = lambdas[plane]
     factor = score_scale * math.log2(math.e)
 
@@ -518,65 +538,99 @@
         )
         heads_done[number] = scaled.astype(jnp.bfloat16)
 
-    def send_attended():
-        for step in range(1, groups):
-            back.append(
-                copies.new(
-                    heads_done.at[ahead[step]], heads_back.at[plane], at_plane(ahead[step])
-                )
-            )
+    def attended_copy(number, source):
+        return pltpu.make_async_remote_copy(
+            src_ref=heads_done.at[number],
+            dst_ref=heads_back.at[source],
+            send_sem=back_send_sems.at[number],
+            recv_sem=back_recv_sems.at[source],
+            device_id=at_plane(number),
+            device_id_type=pl.DeviceIdType.MESH,
+        )
+
+    def attend_and_send(number):
+        attend(number)
+
+        @pl.when(plane != number)
+        def _():
+            attended_copy(number, plane).start()
 
     groups_in_half = 4
     spread(0)
     cross_heads(0)
-    for step in range(1, groups):
-        send_heads(step)
+    send_heads(1)
+    send_heads(2)
+    send_heads(3)
+    spread(1)
     forward(0)
-    spread(1)
-    compute(0)
+    spread(2)
     forward(1)
-    spread(2)
-    reduce_corner(0)
+    pass_corner(0)
+    cross_heads(1)
+    spread(3)
+    forward(2)
+    pass_corner(1)
+    for load in loads[4:]:
+        load.wait()
     compute(1)
-    cross_heads(1)
-    forward(2)
-    reduce_sides(0)
-    spread(3)
+    forward(3)
+    cross_heads(2)
+    pass_corner(2)
+    compute(2)
     reduce_corner(1)
-    compute(2)
-    cross_heads(2)
-    forward(3)
-    finish(0)
-    reduce_sides(1)
-    reduce_corner(2)
+    pass_corner(3)
     cross_heads(3)
     compute(3)
-    finish(1)
+    reduce_corner(2)
+    reduce_sides(1)
+    compute(0)
+    reduce_corner(3)
     reduce_sides(2)
     ready_heads()
-    attend(0)
-    reduce_corner(3)
-    attend(1)
+    attend_and_send(0)
+    attend_and_send(1)
+    finish(1)
+    reduce_corner(0)
+    reduce_sides(3)
+    attend_and_send(2)
     finish(2)
-    reduce_sides(3)
-    attend(2)
+    reduce_sides(0)
+    attend_and_send(3)
     finish(3)
-    attend(3)
-    send_attended()
+    finish(0)
     for copy in homed:
         copy.wait_recv()
     gathered = returned[...].reshape(own_count, model_width)
-    moe_out[...] = jnp.dot(slots, gathered, preferred_element_type=jnp.float32).astype(
-        jnp.bfloat16
-    )
-    for copy in back:
-        copy.wait_recv()
+    moe_out[...] = lax.dot_general(
+        slots, gathered, (((0,), (0,)), ((), ())), preferred_element_type=jnp.float32
+    ).astype(jnp.bfloat16)
+    for number in range(groups):
+
+        @pl.when(plane != number)
+        def _(number=number):
+            attended_copy(number, number).wait_recv()
+
     for number in range(groups):
         columns = slice(number * head_width, (number + 1) * head_width)
         attn_out[:, columns] = jnp.where(
             plane == number, heads_done[number], heads_back[number]
         )
+    for number in range(groups):
+
+        @pl.when(plane != number)
+        def _(number=number):
+            attended_copy(number, plane).wait_send()
+
     copies.drain()
+
+
+def store_kernel(attn_in, moe_in, attn_out, moe_out, sems):
+    pairs = ((attn_in, attn_out), (moe_in, moe_out))
+    stores = [pltpu.make_async_copy(a, b, sems.at[n]) for n, (a, b) in enumerate(pairs)]
+    for store in stores:
+        store.start()
+    for store in stores:
+        store.wait()
 
 
 def fused_local(
@@ -601,21 +655,19 @@
     own_count = moe_input.shape[0] // lax.axis_size("tp")
     hidden_width = w_gate.shape[2]
     chunk = own_count // groups
-    router = jnp.concatenate([group_router, expert_router], axis=1)
-    router = jnp.pad(router, ((0, 0), (0, -router.shape[1] % 128)))
     bf16, f32 = jnp.bfloat16, jnp.float32
     vmem = pl.BlockSpec(memory_space=pltpu.VMEM)
     smem = pl.BlockSpec(memory_space=pltpu.SMEM)
     hbm = pl.BlockSpec(memory_space=pl.ANY)
     copy_count = 3 + 9 + 8 * groups + 5 * groups + 3 + 8 + 3
     blocks = 2 * groups
-    return pl.pallas_call(
+    results = pl.pallas_call(
         functools.partial(fused_kernel, groups, (head_width // 2) ** -0.5),
         out_shape=(
             jax.ShapeDtypeStruct((token_block, width), bf16),
             jax.ShapeDtypeStruct((own_count, model_width), bf16),
         ),
-        in_specs=[hbm, hbm, hbm, smem, vmem, hbm, vmem, vmem, vmem, hbm, hbm, hbm],
+        in_specs=[hbm, hbm, hbm, smem, vmem, hbm] + [vmem] * 4 + [hbm] * 3,
         out_specs=(vmem, vmem),
         scratch_shapes=[
             pltpu.VMEM((own_count, model_width), bf16),
@@ -638,9 +690,12 @@
             pltpu.VMEM((blocks, token_block, head_width), bf16),
             pltpu.VMEM((groups, token_block, head_width), bf16),
             pltpu.VMEM((groups, token_block, head_width), bf16),
+            pltpu.VMEM((128, model_width), bf16),
             pltpu.SemaphoreType.DMA((7,)),
             pltpu.SemaphoreType.DMA((copy_count,)),
             pltpu.SemaphoreType.DMA((copy_count,)),
+            pltpu.SemaphoreType.DMA((groups,)),
+            pltpu.SemaphoreType.DMA((groups,)),
         ],
         compiler_params=pltpu.CompilerParams(
             collective_id=0, has_side_effects=True, vmem_limit_bytes=62_000_000
@@ -653,12 +708,20 @@
         head_gain[None, :],
         moe_input,
         ffn_gain[None, :],
-        router,
-        routes,
+        group_router.T,
+        expert_router.T,
+        routes.T,
         w_gate,
         w_up,
         w_down,
     )
+    return pl.pallas_call(
+        store_kernel,
+        out_shape=tuple(jax.ShapeDtypeStruct(r.shape, r.dtype) for r in results),
+        in_specs=[vmem, vmem],
+        out_specs=(hbm, hbm),
+        scratch_shapes=[pltpu.SemaphoreType.DMA((2,))],
+    )(*results)
 
 
 def chosen_local(*arguments):

time: 78.2 us -> 67.1 us (0.86)
  local copies, waits for them, and re-layouts: 6.29 us -> 0 us
  Pallas kernels: 70.1 us -> 66 us
    pallas_call x1, Pallas kernels: 70.1 us -> 64 us  [fused_local(): pl.pallas_call(functools.partial(fused_kernel, groups, (head_width // 2)...]
    unnamed x3 -> x0, local copies, waits for them, and re-layouts: 5.09 us -> none
    pallas_call x0 -> x1, Pallas kernels: none -> 2.02 us  [fused_local(): pl.pallas_call(store_kernel, out_shape=tuple((jax.ShapeDtypeStruct(r.shap...]
    pad x1 -> x0, local copies, waits for them, and re-layouts: 0.9 us -> none  [fused_local(): router = jnp.pad(router, ((0, 0), (0, -router.shape[1] % 128)))]
    concatenate x1 -> x0, other arithmetic: 0.78 us -> none  [fused_local(): router = jnp.concatenate([group_router, expert_router], axis=1)]
where the time goes in v2:
time: 67.1 us; the launch traced here: 66.6 us
  Pallas kernels  66 us (98%)
    pallas_call x1, Pallas kernels, fused_local(): pl.pallas_call(functools.partial(fused_kernel, groups, (head_width // 2)...  64 us
    pallas_call x1, Pallas kernels, fused_local(): pl.pallas_call(store_kernel, out_shape=tuple((jax.ShapeDtypeStruct(r.shap...  2.02 us

profile of v2, /device:TPU:0, one launch (start us, length us, event | category | flops | bytes accessed | tf_op | source)
XLA Modules:
  0.0 66.6 jit_solution(11493561273274835959)
XLA Ops:
  0.6 64.0 %shard_map.140 = (bf16[256,512]{1,0:T(8,128)(2,1)}, bf16[128,2048]{1,0:T(8,128)(2,1)}) custom-call(bf16[256,512]{1,0:T(8,128)(2,1)} %queries.1, bf16[256,512]{1,0:T(8,128)(2,1)} %keys.1, bf16[256,512]{1,0:T(8,128)(2,1)} %values.1, f32[4]{0:T(128)} %lambdas.1, f32[1,128]{1,0:T(1,128)} %bitcast.9, bf16[512,2048]{1,0:T(8,128)(2,1)} %moe_input.1, ...), custom_call_target="tpu_custom_call" | custom-call | tf_op jit(solution)/shard_map/pallas_call | solution.py:664
  64.6 2.0 %shard_map.141 = (bf16[256,512]{1,0:T(8,128)(2,1)}, bf16[128,2048]{1,0:T(8,128)(2,1)}) custom-call(bf16[256,512]{1,0:T(8,128)(2,1)} %get-tuple-element.4.attn_in, bf16[128,2048]{1,0:T(8,128)(2,1)} %get-tuple-element.5.moe_in), custom_call_target="tpu_custom_call" | custom-call | tf_op jit(solution)/shard_map/pallas_call | solution.py:718
